TPU v7x, 32 devices: a whole 2x2x4 slice. The times are simulated.
32 devices in a mesh: grp: 2 (over y), ep: 4 (over z), tp: 4 (over x, core).
Axes of the slice: x: 2, y: 2, z: 4, core: 2. Of those that a mesh axis runs over, the one named last changes fastest.
Arguments:
- queries: bfloat16 [1024, 1024], P(('grp', 'ep'), 'tp'), parts along dimension 0, may hold values from -6 to 6
- keys: bfloat16 [1024, 1024], P(('grp', 'ep'), 'tp'), parts along dimension 0, may hold values from -6 to 6
- values: bfloat16 [1024, 1024], P(('grp', 'ep'), 'tp'), parts along dimension 0, may hold values from -6 to 6
- lambdas: float32 [8], P('tp'), may hold values from 0.3 to 0.8
- head_gain: float32 [128], replicated, may hold values from 0.1 to 1.9
- tokens: bfloat16 [2048, 1536], P(('grp', 'ep')), parts along dimension 0, may hold values from -6 to 6
- route_ids: int32 [2048, 2], P(('grp', 'ep')), parts along dimension 0, may hold values from 0 to 3, all different within a row; in each aligned block of 256 rows (0 to 255, 256 to 511, ...) at most 256 rows name the same one
- route_weights: float32 [2048, 2], P(('grp', 'ep')), parts along dimension 0, may hold values from 0.2 to 1
- moe_gain: float32 [1536], replicated, may hold values from 0.1 to 1.9
- w_gate: bfloat16 [4, 1536, 3072], P('ep', None, 'tp'), may hold values from -0.15625 to 0.15625
- w_up: bfloat16 [4, 1536, 3072], P('ep', None, 'tp'), may hold values from -0.15625 to 0.15625
- w_down: bfloat16 [4, 3072, 1536], P('ep', 'tp'), may hold values from -0.109375 to 0.109375
Outputs:
- heads_out: bfloat16 [1024, 1024], P(('grp', 'ep'), 'tp'), parts along dimension 0
- expert_out: bfloat16 [2048, 1536], P(('grp', 'ep'), 'tp'), parts along dimension 0
There are 2 independent parts, one for each index of `grp`. A program takes and returns all parts, laid end to end along the dimension named above; an argument that names none is the same for every part. Nothing has to cross between parts.
Inputs may be any that keep to these rules, and one draw needn't show every extreme that they name: `route_ids`: each row names 2 different experts. In the 256 rows of one device no expert is named more than 256 times, and in every draw some device names some expert exactly 256 times.
All inputs are finite; a program needn't handle non-finite values.
Results may differ from a plain program's by a relative error of at most 0.015.
Values may be sent and summed in bfloat16 or wider, within the bound.
A program may use at most 64 MiB of HBM per device.

v0:
```python
import jax
import jax.numpy as jnp
from jax import lax
from jax.sharding import PartitionSpec as P


def attend(queries, keys, values, lambdas, head_gain):
    row_count = queries.shape[0]
    head_count = lambdas.shape[0]
    head_dim = queries.shape[1] // (2 * head_count)
    value_dim = values.shape[1] // head_count
    query_parts = queries.reshape(row_count, head_count, 2, head_dim)
    score_scale = head_dim ** (-0.5)
    running = jnp.full((head_count, 2, row_count), -1e30, jnp.float32)
    key_piece = lax.all_gather(keys, "ep", axis=0, tiled=True)
    value_piece = lax.all_gather(values, "ep", axis=0, tiled=True)
    count = key_piece.shape[0]
    key_parts = key_piece.reshape(count, head_count, 2, head_dim)
    value_parts = value_piece.reshape(count, head_count, value_dim)
    scores = (
        jnp.einsum("qhcd,khcd->hcqk", query_parts, key_parts, preferred_element_type=jnp.float32)
        * score_scale
    )
    newest = jnp.maximum(running, jnp.max(scores, axis=-1))
    weights_now = jnp.exp(scores - newest[..., None])
    totals = jnp.sum(weights_now, axis=-1)
    sums = jnp.einsum(
        "hcqk,khe->hcqe",
        weights_now.astype(jnp.bfloat16),
        value_parts,
        preferred_element_type=jnp.float32,
    )
    running, totals, sums = (newest, totals, sums)
    means = sums / totals[..., None]
    mixed = means[:, 0] - lambdas[:, None, None] * means[:, 1]
    scaled = mixed * lax.rsqrt(jnp.mean(mixed * mixed, axis=-1, keepdims=True) + 1e-06) * head_gain
    return (
        jnp.transpose(scaled, (1, 0, 2))
        .reshape(row_count, head_count * value_dim)
        .astype(jnp.bfloat16)
    )


def experts(tokens, route_ids, route_weights, moe_gain, w_gate, w_up, w_down):
    row_count, width = tokens.shape
    top_count = route_ids.shape[1]
    ep_size = lax.axis_size("ep")
    tp_size = lax.axis_size("tp")
    expert_count = w_gate.shape[0] * ep_size
    capacity = 2 * row_count * top_count // expert_count
    token_float = tokens.astype(jnp.float32)
    normed = (
        token_float
        * lax.rsqrt(jnp.mean(token_float * token_float, axis=1, keepdims=True) + 1e-06)
        * moe_gain
    ).astype(jnp.bfloat16)
    flat_ids = route_ids.reshape(-1)
    onehot = (flat_ids[:, None] == jnp.arange(expert_count, dtype=jnp.int32)[None, :]).astype(
        jnp.int32
    )
    earlier = jnp.cumsum(onehot, axis=0) - onehot
    position = jnp.sum(earlier * onehot, axis=1)
    slot_index = flat_ids * capacity + position
    owners = (
        jnp.full((expert_count * capacity,), row_count, jnp.int32)
        .at[slot_index]
        .set(jnp.arange(row_count * top_count, dtype=jnp.int32) // top_count)
    )
    padded = jnp.concatenate([normed, jnp.zeros((1, width), jnp.bfloat16)], axis=0)
    outgoing = padded[owners].reshape(expert_count, capacity, width)
    gate_mat = w_gate[0]
    up_mat = w_up[0]
    down_mat = w_down[0]
    slice_width = width // tp_size
    own_columns = lax.dynamic_slice_in_dim(
        outgoing, lax.axis_index("tp") * slice_width, slice_width, 2
    )
    arrived = lax.all_to_all(own_columns, "ep", split_axis=0, concat_axis=0, tiled=True)
    piece = lax.all_gather(arrived, "tp", axis=2, tiled=True)
    gate = jnp.einsum("scd,df->scf", piece, gate_mat, preferred_element_type=jnp.float32)
    upward = jnp.einsum("scd,df->scf", piece, up_mat, preferred_element_type=jnp.float32)
    hidden = (jax.nn.silu(gate) * upward).astype(jnp.bfloat16)
    flat_hidden = hidden.reshape(-1, hidden.shape[2])
    summed = lax.psum_scatter(
        jnp.einsum("fd,sf->ds", down_mat, flat_hidden, preferred_element_type=jnp.float32).astype(
            jnp.bfloat16
        ),
        "tp",
        scatter_dimension=0,
        tiled=True,
    )
    back = lax.all_to_all(summed, "ep", split_axis=1, concat_axis=1, tiled=True)
    picked = (
        jnp.take(back, slot_index, axis=1).astype(jnp.float32).reshape(-1, row_count, top_count)
    )
    combined = jnp.einsum("drk,rk->rd", picked, route_weights)
    return combined.astype(jnp.bfloat16)


def on_device(
    queries,
    keys,
    values,
    lambdas,
    head_gain,
    tokens,
    route_ids,
    route_weights,
    moe_gain,
    w_gate,
    w_up,
    w_down,
):
    heads_out = attend(queries, keys, values, lambdas, head_gain)
    expert_out = experts(tokens, route_ids, route_weights, moe_gain, w_gate, w_up, w_down)
    return (heads_out, expert_out)


def solution(mesh):
    in_specs = (
        P(("grp", "ep"), "tp"),
        P(("grp", "ep"), "tp"),
        P(("grp", "ep"), "tp"),
        P("tp"),
        P(),
        P(("grp", "ep"), None),
        P(("grp", "ep"), None),
        P(("grp", "ep"), None),
        P(),
        P("ep", None, "tp"),
        P("ep", None, "tp"),
        P("ep", "tp", None),
    )
    out_specs = (P(("grp", "ep"), "tp"), P(("grp", "ep"), "tp"))
    return jax.shard_map(
        on_device, mesh=mesh, in_specs=in_specs, out_specs=out_specs, check_vma=False
    )
```

profile of v0, /device:TPU:0, one launch (start us, length us, event | category | flops | bytes accessed | tf_op | source)
XLA Modules:
  0.0 183.2 jit_solution(15858981580019613275)
XLA Ops:
  7.2 1.0 copy.40
  8.5 0.7 broadcast_multiply_fusion
  9.2 1.2 reduce-window.6
  10.4 0.2 slice_reduce_fusion
  10.6 0.2 reduce-window.9
  11.2 2.4 %scatter_custom_fusion = s32[1024]{0:T(1024)S(1)} fusion(s32[512]{0:T(512)S(1)} %bitcast.95, s32[512]{0:T(512)S(1)} %add_select_fusion, s32[]{:T(128)} %constant.33.clone.1), kind=kCustom, calls=%fused_computation.53 | custom fusion | bytes 4100 | tf_op jit(solution)/shard_map/scatter | solution.py:67
  13.7 1.4 fusion.8
  15.1 1.4 fusion.10
  16.5 5.6 %gather_fusion = bf16[1024,1536]{1,0:T(8,128)(2,1)} fusion(bf16[257,1536]{1,0:T(8,128)(2,1)S(1)} %concatenate.3, s32[1024]{0:T(1024)S(1)} %fusion.23), kind=kCustom, calls=%fused_computation | custom fusion | bytes 6295552 | tf_op jit(solution)/shard_map/gather | solution.py:70
  22.1 1.2 constant_dynamic-slice_fusion
  23.3 26.4 %all_to_all.17 = bf16[4,256,384]{2,1,0:T(8,128)(2,1)} all-to-all(bf16[4,256,384]{2,1,0:T(8,128)(2,1)S(1)} %constant_dynamic-slice_fusion), channel_id=1, replica_groups=mesh['grp'=2,'ep'=4,'tp'=4] {'ep'}, dimensions={0} | all-to-all | bytes 1572864 | tf_op jit(solution)/shard_map/all_to_all | solution.py:78
  49.8 27.7 %all-gather.2.cloned.1.call-done = bf16[4,256,1536]{2,1,0:T(8,128)(2,1)} async-done(((bf16[4,256,384]{2,1,0:T(8,128)(2,1)}), bf16[4,256,1536]{2,1,0:T(8,128)(2,1)}) %all-gather.2.cloned.1.call-update) | async-done | bytes 3145744 | tf_op jit(solution)/shard_map/all_gather | solution.py:79
  77.5 5.4 %fusion.2 = f32[4,256,768]{2,1,0:T(8,128)S(1)} fusion(bf16[4,256,1536]{2,1,0:T(8,128)(2,1)} %all-gather.2.cloned.1.call-done, bf16[1,1536,768]{2,1,0:T(8,128)(2,1)} %param.22), kind=kOutput, calls=%fused_computation.7 | convolution fusion | flops 2415919104 | bytes 8650752 | tf_op jit(solution)/shard_map/scd,df->scf/dot_general | solution.py:81
  82.8 2.9 %multiply_convert_fusion = bf16[4,256,768]{2,1,0:T(8,128)(2,1)S(1)} fusion(f32[4,256,768]{2,1,0:T(8,128)S(1)} %fusion.2, bf16[4,256,1536]{2,1,0:T(8,128)(2,1)S(1)} %copy-done.8, bf16[1,1536,768]{2,1,0:T(8,128)(2,1)S(1)} %copy-done.9), kind=kOutput, calls=%fused_computation.5 | convolution fusion | flops 2420637696 | bytes 10223616 | tf_op jit(solution)/shard_map/scd,df->scf/dot_general | solution.py:80
  85.8 4.0 %fusion = bf16[1536,1024]{0,1:T(8,128)(2,1)} fusion(bf16[1024,768]{1,0:T(8,128)(2,1)S(1)} %bitcast.99, bf16[1,768,1536]{2,1,0:T(8,128)(2,1)S(1)} %copy-done), kind=kOutput, calls=%fused_computation.4 | convolution fusion | flops 2417491968 | bytes 7077888 | tf_op jit(solution)/shard_map/fd,sf->ds/dot_general | solution.py:85
  89.8 4.6 %copy.49 = bf16[1536,1024]{1,0:T(8,128)(2,1)} copy(bf16[1536,1024]{0,1:T(8,128)(2,1)} %fusion) | data formatting | bytes 6291456
  94.7 0.4 copy-done.4
  95.1 0.8 copy.43
  95.9 0.8 copy.47
  96.7 13.9 %all_gather.9 = bf16[512,256]{1,0:T(8,128)(2,1)S(1)} all-gather(bf16[128,256]{1,0:T(8,128)(2,1)S(1)} %copy-done.1), channel_id=1, replica_groups=mesh['grp'=2,'ep'=4,'tp'=4] {'ep'}, dimensions={0}, use_global_device_ids=true | all-gather | bytes 327680 | tf_op jit(solution)/shard_map/all_gather | solution.py:15
  110.9 1.3 fusion.30
  112.2 20.3 %reduce-scatter.4.cloned.1.call-done = bf16[384,1024]{1,0:T(8,128)(2,1)} async-done(((bf16[1536,1024]{1,0:T(8,128)(2,1)}), bf16[384,1024]{1,0:T(8,128)(2,1)}) %reduce-scatter.4.cloned.1.call-update) | async-done | bytes 786448
  132.5 2.3 %copy.50 = bf16[384,1024]{0,1:T(8,128)(2,1)} copy(bf16[384,1024]{1,0:T(8,128)(2,1)} %reduce-scatter.4.cloned.1.call-done) | data formatting | bytes 1572864
  134.8 4.7 %all-to-all-start.1 = ((bf16[384,4,256]{0,2,1:T(8,128)(2,1)}), bf16[384,4,256]{0,2,1:T(8,128)(2,1)S(1)}, u32[]{:S(2)}, u32[]{:S(2)}) async-start(bf16[384,4,256]{0,2,1:T(8,128)(2,1)} %bitcast.87), calls=%async_computation.1 | async-start | bytes 1572864 | tf_op jit(solution)/shard_map/all_to_all | solution.py:92
  139.5 27.2 %all_gather.10 = bf16[512,256]{1,0:T(8,128)(2,1)S(1)} all-gather(bf16[128,256]{1,0:T(8,128)(2,1)S(1)} %copy-done.2), channel_id=1, replica_groups=mesh['grp'=2,'ep'=4,'tp'=4] {'ep'}, dimensions={0}, use_global_device_ids=true | all-gather | bytes 327680 | tf_op jit(solution)/shard_map/all_gather | solution.py:16
  166.7 0.9 copy.38
  167.6 1.5 fusion.11
  169.1 1.7 convolution_divide_fusion
  171.1 0.7 copy.45
  171.8 1.9 %gather_fusion.1 = bf16[512,384]{1,0:T(8,128)(2,1)S(1)} fusion(bf16[384,1024]{0,1:T(8,128)(2,1)S(1)} %bitcast.85, s32[1024]{0:T(1024)S(1)} %pad_clamp_fusion), kind=kCustom, calls=%fused_computation.1 | custom fusion | bytes 788480 | tf_op jit(solution)/shard_map/jit(_take)/gather | solution.py:94
  173.9 1.7 fusion.15
  175.7 0.7 copy.55
  (47 shorter events, 1.8 us)
Async XLA Ops:
  7.2 78.6 %copy-start = (bf16[1,768,1536]{2,1,0:T(8,128)(2,1)S(1)}, bf16[1,768,1536]{2,1,0:T(8,128)(2,1)}, u32[]{:S(2)}) copy-start(bf16[1,768,1536]{2,1,0:T(8,128)(2,1)} %param.23) | copy-start | bytes 7077892
  7.2 70.3 %all-gather.2.cloned.1.call-start = ((), (), s32[]{:S(2)}) async-start(), calls=%async_computation.3 | async-start | bytes 3932160 | tf_op jit(solution)/shard_map/all_gather | solution.py:79
  49.7 82.8 %reduce-scatter.4.cloned.1.call-start = ((), (), s32[]{:S(2)}) async-start(), calls=%async_computation.4 | async-start | bytes 3932160
  77.4 5.4 %copy-start.8 = (bf16[4,256,1536]{2,1,0:T(8,128)(2,1)S(1)}, bf16[4,256,1536]{2,1,0:T(8,128)(2,1)}, u32[]{:S(2)}) copy-start(bf16[4,256,1536]{2,1,0:T(8,128)(2,1)} %all-gather.2.cloned.1.call-done) | copy-start | bytes 9437188
  77.4 5.4 %copy-start.9 = (bf16[1,1536,768]{2,1,0:T(8,128)(2,1)S(1)}, bf16[1,1536,768]{2,1,0:T(8,128)(2,1)}, u32[]{:S(2)}) copy-start(bf16[1,1536,768]{2,1,0:T(8,128)(2,1)} %param.21) | copy-start | bytes 7077892
  94.4 0.7 copy-start.4
  94.4 1.4 copy-start.5
  94.4 2.3 %copy-start.1 = (bf16[128,256]{1,0:T(8,128)(2,1)S(1)}, bf16[128,256]{1,0:T(8,128)(2,1)}, u32[]{:S(2)}) copy-start(bf16[128,256]{1,0:T(8,128)(2,1)} %param.13) | copy-start | bytes 196612
  94.4 16.4 %copy-start.3 = (bf16[128,256]{1,0:T(8,128)(2,1)S(1)}, bf16[128,256]{1,0:T(8,128)(2,1)}, u32[]{:S(2)}) copy-start(bf16[128,256]{1,0:T(8,128)(2,1)} %param.12) | copy-start | bytes 196612
  94.5 45.1 %copy-start.2 = (bf16[128,256]{1,0:T(8,128)(2,1)S(1)}, bf16[128,256]{1,0:T(8,128)(2,1)}, u32[]{:S(2)}) copy-start(bf16[128,256]{1,0:T(8,128)(2,1)} %param.14) | copy-start | bytes 196612
  112.2 58.6 %copy-start.6 = (f32[2]{0:T(128)S(1)}, f32[2]{0:T(128)}, u32[]{:S(2)}) copy-start(f32[2]{0:T(128)} %param.15) | copy-start | bytes 28
  134.8 36.2 %copy-start.7 = (f32[128]{0:T(128)S(1)}, f32[128]{0:T(128)}, u32[]{:S(2)}) copy-start(f32[128]{0:T(128)} %param.16) | copy-start | bytes 1540
  134.8 37.1 %all-to-all-start.1 = ((bf16[384,4,256]{0,2,1:T(8,128)(2,1)}), bf16[384,4,256]{0,2,1:T(8,128)(2,1)S(1)}, u32[]{:S(2)}, u32[]{:S(2)}) async-start(bf16[384,4,256]{0,2,1:T(8,128)(2,1)} %bitcast.87), calls=%async_computation.1 | async-start | bytes 1572864 | tf_op jit(solution)/shard_map/all_to_all | solution.py:92
Sparse Core Ops, SparseCore 0:
  49.8 27.5 all-gather.1
  94.6 37.8 reduce-scatter.3
where the time goes:
time: 184 us; the launch traced here: 183 us
  blocking collectives  67.5 us (37%)
  waiting for transfers between devices  48 us (26%)
  local copies, waits for them, and re-layouts  24.9 us (14%)
  matrix products  17 us (9%)
  between operations  14.3 us (8%)
  other arithmetic  6.72 us (4%)
  starting transfers between devices  4.81 us (3%)
    all_gather x1, waiting for transfers between devices, experts(): piece = lax.all_gather(arrived, 'tp', axis=2, tiled=True)  27.7 us
    all_gather x1, blocking collectives, attend(): value_piece = lax.all_gather(values, 'ep', axis=0, tiled=True)  27.2 us
    all_to_all x1, blocking collectives, experts(): lax.all_to_all(own_columns, 'ep', split_axis=0, concat_axis=0, tiled=True)  26.4 us
    unnamed x3, waiting for transfers between devices  20.3 us
    all_gather x1, blocking collectives, attend(): key_piece = lax.all_gather(keys, 'ep', axis=0, tiled=True)  13.9 us
    unnamed x26, local copies, waits for them, and re-layouts  10 us
    gather x1, local copies, waits for them, and re-layouts, experts(): outgoing = padded[owners].reshape(expert_count, capacity, width)  5.61 us
    dot_general x1, matrix products, experts(): jnp.einsum('scd,df->scf', piece, up_mat, preferred_element_type=jnp.float32)  5.36 us
  transfers between devices with their start and end apart: 3, of which 2 were waited for; matrix products, arithmetic and copies ran while one was open for 5% of the time, Pallas kernels for 0%

commit v1 on v0

--- a/solution.py
+++ b/solution.py
@@ -12,8 +12,11 @@
     query_parts = queries.reshape(row_count, head_count, 2, head_dim)
     score_scale = head_dim ** (-0.5)
     running = jnp.full((head_count, 2, row_count), -1e30, jnp.float32)
-    key_piece = lax.all_gather(keys, "ep", axis=0, tiled=True)
-    value_piece = lax.all_gather(values, "ep", axis=0, tiled=True)
+    key_piece, value_piece = jnp.split(
+        lax.all_gather(jnp.concatenate([keys, values], axis=1), "ep", axis=0, tiled=True),
+        [keys.shape[1]],
+        axis=1,
+    )
     count = key_piece.shape[0]
     key_parts = key_piece.reshape(count, head_count, 2, head_dim)
     value_parts = value_piece.reshape(count, head_count, value_dim)

time: 184 us -> 171 us (0.929)
  blocking collectives: 67.5 us -> 42.4 us
  waiting for transfers between devices: 48 us -> 60.7 us
    all_gather x2 -> x1, blocking collectives: 41.2 us -> 16 us  [attend(): lax.all_gather(jnp.concatenate([keys, values], axis=1), 'ep', axis=0, til...]
    all_to_all x1, waiting for transfers between devices: 0.01 us -> 13.5 us  [experts(): back = lax.all_to_all(summed, 'ep', split_axis=1, concat_axis=1, tiled=True)]
  transfers between devices with their start and end apart: 3 -> 3, of which waited for: 2 -> 3; matrix products, arithmetic and copies ran while one was open for 5% -> 5% of each run, Pallas kernels for 0% -> 0%
where the time goes in v1:
time: 171 us
  waiting for transfers between devices  60.7 us (35%)
  blocking collectives  42.4 us (25%)
  local copies, waits for them, and re-layouts  25.1 us (15%)
  matrix products  17 us (10%)
  between operations  14.3 us (8%)
  other arithmetic  6.59 us (4%)
  starting transfers between devices  4.68 us (3%)
    all_gather x1, waiting for transfers between devices, experts(): piece = lax.all_gather(arrived, 'tp', axis=2, tiled=True)  27.7 us
    all_to_all x1, blocking collectives, experts(): lax.all_to_all(own_columns, 'ep', split_axis=0, concat_axis=0, tiled=True)  26.4 us
    unnamed x3, waiting for transfers between devices  19.5 us
    all_gather x1, blocking collectives, attend(): lax.all_gather(jnp.concatenate([keys, values], axis=1), 'ep', axis=0, til...  16 us
    all_to_all x1, waiting for transfers between devices, experts(): back = lax.all_to_all(summed, 'ep', split_axis=1, concat_axis=1, tiled=True)  13.5 us
    unnamed x26, local copies, waits for them, and re-layouts  10.2 us
    gather x1, local copies, waits for them, and re-layouts, experts(): outgoing = padded[owners].reshape(expert_count, capacity, width)  5.61 us
    dot_general x1, matrix products, experts(): jnp.einsum('scd,df->scf', piece, up_mat, preferred_element_type=jnp.float32)  5.36 us
  transfers between devices with their start and end apart: 3, of which 3 were waited for; matrix products, arithmetic and copies ran while one was open for 5% of the time, Pallas kernels for 0%

profile of v1, /device:TPU:0, one launch (start us, length us, event | category | flops | bytes accessed | tf_op | source)
XLA Modules:
  0.0 170.7 jit_solution(8142326767872531657)
XLA Ops:
  7.2 1.0 copy.44
  8.5 0.7 broadcast_multiply_fusion
  9.2 1.2 reduce-window.6
  10.4 0.2 slice_reduce_fusion
  10.6 0.2 reduce-window.9
  11.2 2.4 %scatter_custom_fusion = s32[1024]{0:T(1024)S(1)} fusion(s32[512]{0:T(512)S(1)} %bitcast.97, s32[512]{0:T(512)S(1)} %add_select_fusion, s32[]{:T(128)} %constant.33.clone.1), kind=kCustom, calls=%fused_computation.55 | custom fusion | bytes 4100 | tf_op jit(solution)/shard_map/scatter | solution.py:70
  13.7 1.4 fusion.8
  15.1 1.4 fusion.10
  16.5 5.6 %gather_fusion = bf16[1024,1536]{1,0:T(8,128)(2,1)} fusion(bf16[257,1536]{1,0:T(8,128)(2,1)S(1)} %concatenate.7, s32[1024]{0:T(1024)S(1)} %fusion.24), kind=kCustom, calls=%fused_computation | custom fusion | bytes 6295552 | tf_op jit(solution)/shard_map/gather | solution.py:73
  22.1 1.2 constant_dynamic-slice_fusion
  23.3 26.4 %all_to_all.17 = bf16[4,256,384]{2,1,0:T(8,128)(2,1)} all-to-all(bf16[4,256,384]{2,1,0:T(8,128)(2,1)S(1)} %constant_dynamic-slice_fusion), channel_id=1, replica_groups=mesh['grp'=2,'ep'=4,'tp'=4] {'ep'}, dimensions={0} | all-to-all | bytes 1572864 | tf_op jit(solution)/shard_map/all_to_all | solution.py:81
  49.8 27.7 %all-gather.2.cloned.1.call-done = bf16[4,256,1536]{2,1,0:T(8,128)(2,1)} async-done(((bf16[4,256,384]{2,1,0:T(8,128)(2,1)}), bf16[4,256,1536]{2,1,0:T(8,128)(2,1)}) %all-gather.2.cloned.1.call-update) | async-done | bytes 3145744 | tf_op jit(solution)/shard_map/all_gather | solution.py:82
  77.5 5.4 %fusion.2 = f32[4,256,768]{2,1,0:T(8,128)S(1)} fusion(bf16[4,256,1536]{2,1,0:T(8,128)(2,1)} %all-gather.2.cloned.1.call-done, bf16[1,1536,768]{2,1,0:T(8,128)(2,1)} %param.22), kind=kOutput, calls=%fused_computation.7 | convolution fusion | flops 2415919104 | bytes 8650752 | tf_op jit(solution)/shard_map/scd,df->scf/dot_general | solution.py:84
  82.8 2.9 %multiply_convert_fusion = bf16[4,256,768]{2,1,0:T(8,128)(2,1)S(1)} fusion(f32[4,256,768]{2,1,0:T(8,128)S(1)} %fusion.2, bf16[4,256,1536]{2,1,0:T(8,128)(2,1)S(1)} %copy-done.8, bf16[1,1536,768]{2,1,0:T(8,128)(2,1)S(1)} %copy-done.9), kind=kOutput, calls=%fused_computation.5 | convolution fusion | flops 2420637696 | bytes 10223616 | tf_op jit(solution)/shard_map/scd,df->scf/dot_general | solution.py:83
  85.8 4.0 %fusion = bf16[1536,1024]{0,1:T(8,128)(2,1)} fusion(bf16[1024,768]{1,0:T(8,128)(2,1)S(1)} %bitcast.101, bf16[1,768,1536]{2,1,0:T(8,128)(2,1)S(1)} %copy-done), kind=kOutput, calls=%fused_computation.4 | convolution fusion | flops 2417491968 | bytes 7077888 | tf_op jit(solution)/shard_map/fd,sf->ds/dot_general | solution.py:88
  89.8 4.6 %copy.54 = bf16[1536,1024]{1,0:T(8,128)(2,1)} copy(bf16[1536,1024]{0,1:T(8,128)(2,1)} %fusion) | data formatting | bytes 6291456
  94.7 0.6 copy-done.2
  95.3 16.0 %all_gather.6 = bf16[512,512]{1,0:T(8,128)(2,1)S(1)} all-gather(bf16[128,512]{1,0:T(8,128)(2,1)S(1)} %pad_maximum_fusion), channel_id=1, replica_groups=mesh['grp'=2,'ep'=4,'tp'=4] {'ep'}, dimensions={0}, use_global_device_ids=true | all-gather | bytes 655360 | tf_op jit(solution)/shard_map/all_gather | solution.py:16
  111.7 1.3 fusion.32
  113.0 19.5 %reduce-scatter.4.cloned.1.call-done = bf16[384,1024]{1,0:T(8,128)(2,1)} async-done(((bf16[1536,1024]{1,0:T(8,128)(2,1)}), bf16[384,1024]{1,0:T(8,128)(2,1)}) %reduce-scatter.4.cloned.1.call-update) | async-done | bytes 786448
  132.5 2.3 %copy.55 = bf16[384,1024]{0,1:T(8,128)(2,1)} copy(bf16[384,1024]{1,0:T(8,128)(2,1)} %reduce-scatter.4.cloned.1.call-done) | data formatting | bytes 1572864
  134.8 4.6 %all-to-all-start.1 = ((bf16[384,4,256]{0,2,1:T(8,128)(2,1)}), bf16[384,4,256]{0,2,1:T(8,128)(2,1)S(1)}, u32[]{:S(2)}, u32[]{:S(2)}) async-start(bf16[384,4,256]{0,2,1:T(8,128)(2,1)} %bitcast.89), calls=%async_computation.1 | async-start | bytes 1572864 | tf_op jit(solution)/shard_map/all_to_all | solution.py:95
  139.4 0.8 copy.47
  140.1 0.8 copy.52
  141.0 0.9 copy.41
  141.8 1.4 fusion.12
  143.2 1.6 convolution_divide_fusion
  145.1 0.7 copy.49
  145.8 13.5 %all-to-all-done.1 = bf16[384,4,256]{0,2,1:T(8,128)(2,1)S(1)} async-done(((bf16[384,4,256]{0,2,1:T(8,128)(2,1)}), bf16[384,4,256]{0,2,1:T(8,128)(2,1)S(1)}, u32[]{:S(2)}, u32[]{:S(2)}) %all-to-all-start.1) | async-done | bytes 786464 | tf_op jit(solution)/shard_map/all_to_all | solution.py:95
  159.3 1.9 %gather_fusion.1 = bf16[512,384]{1,0:T(8,128)(2,1)S(1)} fusion(bf16[384,1024]{0,1:T(8,128)(2,1)S(1)} %bitcast.87, s32[1024]{0:T(1024)S(1)} %pad_clamp_fusion), kind=kCustom, calls=%fused_computation.1 | custom fusion | bytes 788480 | tf_op jit(solution)/shard_map/jit(_take)/gather | solution.py:97
  161.4 1.7 %fusion.16 = bf16[256,1,384]{2,1,0:T(2,128)(2,1)S(1)} fusion(bf16[256,2,1]{1,2,0:T(2,128)(2,1)} %copy.52, bf16[384,256,2]{0,2,1:T(2,128)(2,1)S(1)} %gather.11, pred[256,2]{1,0:T(8,128)(4,1)} %copy.47), kind=kOutput, calls=%fused_computation.25 | convolution fusion | flops 589824 | bytes 591360 | tf_op jit(solution)/shard_map/drk,rk->rd/dot_general | solution.py:99
  163.1 0.7 copy.60
  (48 shorter events, 1.8 us)
Async XLA Ops:
  7.2 78.6 %copy-start = (bf16[1,768,1536]{2,1,0:T(8,128)(2,1)S(1)}, bf16[1,768,1536]{2,1,0:T(8,128)(2,1)}, u32[]{:S(2)}) copy-start(bf16[1,768,1536]{2,1,0:T(8,128)(2,1)} %param.23) | copy-start | bytes 7077892
  7.2 70.3 %all-gather.2.cloned.1.call-start = ((), (), s32[]{:S(2)}) async-start(), calls=%async_computation.3 | async-start | bytes 3932160 | tf_op jit(solution)/shard_map/all_gather | solution.py:82
  49.7 82.8 %reduce-scatter.4.cloned.1.call-start = ((), (), s32[]{:S(2)}) async-start(), calls=%async_computation.4 | async-start | bytes 3932160
  77.4 5.4 %copy-start.8 = (bf16[4,256,1536]{2,1,0:T(8,128)(2,1)S(1)}, bf16[4,256,1536]{2,1,0:T(8,128)(2,1)}, u32[]{:S(2)}) copy-start(bf16[4,256,1536]{2,1,0:T(8,128)(2,1)} %all-gather.2.cloned.1.call-done) | copy-start | bytes 9437188
  77.4 5.4 %copy-start.9 = (bf16[1,1536,768]{2,1,0:T(8,128)(2,1)S(1)}, bf16[1,1536,768]{2,1,0:T(8,128)(2,1)}, u32[]{:S(2)}) copy-start(bf16[1,1536,768]{2,1,0:T(8,128)(2,1)} %param.21) | copy-start | bytes 7077892
  94.4 0.8 copy-start.2
  94.4 0.9 copy-start.3
  94.4 17.1 %copy-start.1 = (bf16[128,256]{1,0:T(8,128)(2,1)S(1)}, bf16[128,256]{1,0:T(8,128)(2,1)}, u32[]{:S(2)}) copy-start(bf16[128,256]{1,0:T(8,128)(2,1)} %param.12) | copy-start | bytes 196612
  94.4 17.2 %copy-start.4 = (s32[256,2]{0,1:T(2,128)S(1)}, s32[256,2]{0,1:T(2,128)}, u32[]{:S(2)}) copy-start(s32[256,2]{0,1:T(2,128)} %param.18) | copy-start | bytes 6148
  111.3 28.8 %copy-start.5 = (f32[256,2]{0,1:T(2,128)S(1)}, f32[256,2]{0,1:T(2,128)}, u32[]{:S(2)}) copy-start(f32[256,2]{0,1:T(2,128)} %param.19) | copy-start | bytes 6148
  113.0 31.9 %copy-start.6 = (f32[2]{0:T(128)S(1)}, f32[2]{0:T(128)}, u32[]{:S(2)}) copy-start(f32[2]{0:T(128)} %param.15) | copy-start | bytes 28
  113.0 32.0 %copy-start.7 = (f32[128]{0:T(128)S(1)}, f32[128]{0:T(128)}, u32[]{:S(2)}) copy-start(f32[128]{0:T(128)} %param.16) | copy-start | bytes 1540
  134.8 24.5 %all-to-all-start.1 = ((bf16[384,4,256]{0,2,1:T(8,128)(2,1)}), bf16[384,4,256]{0,2,1:T(8,128)(2,1)S(1)}, u32[]{:S(2)}, u32[]{:S(2)}) async-start(bf16[384,4,256]{0,2,1:T(8,128)(2,1)} %bitcast.89), calls=%async_computation.1 | async-start | bytes 1572864 | tf_op jit(solution)/shard_map/all_to_all | solution.py:95
Sparse Core Ops, SparseCore 0:
  49.8 27.5 all-gather.1
  94.6 37.8 reduce-scatter.3
